TPU v7x, 512 devices: a whole 4x4x16 slice. The times are simulated.
512 devices in a mesh: sp: 16 (over z), fs: 4 (over y), tp: 8 (over x, core).
Axes of the slice: x: 4, y: 4, z: 16, core: 2. Of those that a mesh axis runs over, the one named last changes fastest.
Arguments:
- input_layer_rows: bfloat16 [4, 4096, 2048], P('fs', 'sp'), may hold values from -6 to 6
- input_norm_gain: float32 [2048], replicated, may hold values from 0.1 to 1.9
- query_weight_attention: bfloat16 [2048, 1024], P(('sp', 'fs'), 'tp'), may hold values from -0.125 to 0.125
- key_weight_attention: bfloat16 [2048, 1024], P(('sp', 'fs'), 'tp'), may hold values from -0.125 to 0.125
- value_weight_attention: bfloat16 [2048, 1024], P(('sp', 'fs'), 'tp'), may hold values from -0.125 to 0.125
- query_weight_recurrent: bfloat16 [2048, 1024], P(('sp', 'fs'), 'tp'), may hold values from -0.125 to 0.125
- forget_weight_recurrent: bfloat16 [2048, 1024], P(('sp', 'fs'), 'tp'), may hold values from -0.125 to 0.125
- value_weight_recurrent: bfloat16 [2048, 1024], P(('sp', 'fs'), 'tp'), may hold values from -0.125 to 0.125
- gate_weight_recurrent: bfloat16 [2048, 1024], P(('sp', 'fs'), 'tp'), may hold values from -0.125 to 0.125
- output_weight_attention: bfloat16 [2048, 1024], P(('sp', 'fs'), 'tp'), may hold values from -0.125 to 0.125
- emitted_projection_linear_scan: bfloat16 [2048, 1024], P(('sp', 'fs'), 'tp'), may hold values from -0.125 to 0.125
- score_offset: float32 [8], P('tp'), as said below
- attention_norm_gain: float32 [1024], P('tp'), may hold values from 0.1 to 1.9
- recurrence_norm_gain: float32 [1024], P('tp'), may hold values from 0.1 to 1.9
- forget_floor: float32 [1024], P('tp'), may hold values from 0.1 to 0.5
- forget_offset: float32 [1024], P('tp'), as said below
- extra_log_decay: float32 [4, 4096, 1024], P('fs', 'sp', 'tp')
Outputs:
- layer_out: bfloat16 [4, 4096, 2048], P('fs', ('sp', 'tp'))
- row_log_total: float32 [4, 8, 4096], P('fs', 'tp', 'sp')
Inputs may be any that keep to these rules, and one draw needn't show every extreme that they name: `score_offset`: each head's offset lies between -ln(4096) - 2 and -ln(4096) + 0.5. `forget_offset`: each channel's offset lies between ln(256) - 3 and ln(4096) + 0.6.
All inputs are finite; a program needn't handle non-finite values.
Results may differ from a plain program's by a relative error of at most 0.015.
Values may be sent and summed in bfloat16 or wider, within the bound.
No kernel may reach another device: no remote copies, remote signals or barrier semaphores. Data moves between devices by JAX's collectives and lax.ppermute only.
A program may use at most 64 MiB of HBM per device.

v0:
```python
import jax
import jax.numpy as jnp
from jax import lax
from jax.sharding import PartitionSpec as P

HEAD = 128
BLOCK = 64


epsilon = 1e-06
log_floor = 0.05


def sent_together(arrays, axis, dim, along):
    ends, at = ([], 0)
    for a in arrays[:-1]:
        at += a.shape[along]
        ends.append(at)
    both = jnp.concatenate(arrays, axis=along)
    return tuple(jnp.split(lax.all_gather(both, axis, axis=dim, tiled=True), ends, axis=along))


def collected_together(shard, axis):
    leaves = jax.tree.leaves(shard)
    turns = sorted(range(len(leaves)), key=lambda k: -leaves[k].size)
    width = (1, *leaves[turns[0]].shape)[-1]
    lines = [
        jnp.pad(leaves[k].reshape(-1), (0, -leaves[k].size % width)).reshape(-1, width)
        for k in turns
    ]
    both, at, found = (lax.all_gather(jnp.concatenate(lines), axis), 0, {})
    for k, line in zip(turns, lines):
        share = both[:, at : at + len(line)].reshape(len(both), -1)
        found[k] = share[:, : leaves[k].size].reshape(-1, *leaves[k].shape)
        at += len(line)
    numbers = iter(range(len(leaves)))
    return jax.tree.map(lambda _: found[next(numbers)], shard)


def entering(shard, axis, combine, identity):
    size, index = (lax.axis_size(axis), lax.axis_index(axis))
    everything = collected_together(
        jax.tree.map(lambda part, kind: part.astype(kind), shard, (jnp.bfloat16, jnp.bfloat16)),
        axis,
    )
    start = jax.tree.map(
        lambda part, zero: jnp.broadcast_to(jnp.asarray(zero, part.dtype), part.shape),
        shard,
        identity,
    )

    def hop(k, before):
        reached = k < index
        new = combine(
            before, jax.tree.map(lambda part, own: part[k].astype(own.dtype), everything, shard)
        )
        return jax.tree.map(lambda a, b: jnp.where(reached, a, b), new, before)

    return lax.fori_loop(0, size, hop, start)


def in_blocks(shard, dim, size):
    before, after = (shard.shape[:dim], shard.shape[dim + 1 :])
    return jnp.moveaxis(shard.reshape(*before, size, -1, *after), dim, 0)


def summed_on_arrival(shard, axis, dim):
    size = lax.axis_size(axis)
    tiles = lax.all_to_all(in_blocks(shard, dim, size), axis, 0, 0, tiled=True)
    return jnp.sum(tiles.astype(jnp.float32), axis=0)


def head_norm(values, gain):
    square_mean = jnp.mean(values * values, axis=-1, keepdims=True)
    return values * lax.rsqrt(square_mean + epsilon) * gain


def recurrence_block(memory_matrix, inputs):
    query_slice, decay_part, key_slice, value_slice = inputs
    highest_score = lax.Precision.HIGHEST
    length = decay_part.shape[0]
    running_total = jnp.cumsum(decay_part, axis=0)
    causal = (
        lax.broadcasted_iota(jnp.int32, (length, length), 0)
        >= lax.broadcasted_iota(jnp.int32, (length, length), 1)
    )[:, :, None, None]
    relative = jnp.where(causal, running_total[:, None] - running_total[None, :], -jnp.inf)
    pairwise = jnp.sum(query_slice[:, None] * key_slice[None, :] * jnp.exp(relative), axis=-1)
    inner_part = jnp.einsum("tsh,shv->thv", pairwise, value_slice, precision=highest_score)
    carried_state = jnp.einsum(
        "fby,bym->fbm", query_slice * jnp.exp(running_total), memory_matrix, precision=highest_score
    )
    final_total = running_total[-1]
    updated_state = jnp.exp(final_total)[:, :, None] * memory_matrix + jnp.einsum(
        "rxc,rxa->xca",
        key_slice * jnp.exp(final_total[None] - running_total),
        value_slice,
        precision=highest_score,
    )
    return (updated_state, inner_part + carried_state)


def stick_piece(queries, shifts, weighted, keep_total, key_value, is_own, is_valid):
    scores = (
        jnp.einsum("thd,shd->hts", queries, key_value[0], preferred_element_type=jnp.float32)
        * HEAD ** (-0.5)
        + shifts[:, None, None]
    )
    logarithmic_retention = jax.nn.log_sigmoid(-scores)
    if is_own:
        rows_here = scores.shape[1]
        strict = lax.broadcasted_iota(jnp.int32, (rows_here, rows_here), 0) > lax.broadcasted_iota(
            jnp.int32, (rows_here, rows_here), 1
        )
        logarithmic_retention = jnp.where(strict, logarithmic_retention, 0.0)
    suffix = lax.cumsum(logarithmic_retention, axis=2, reverse=True) - logarithmic_retention
    log_weight = jax.nn.log_sigmoid(scores) + suffix + keep_total[:, :, None]
    if is_own:
        log_weight = jnp.where(strict, log_weight, -jnp.inf)
    weights = jnp.where(is_valid, jnp.exp(log_weight), 0.0).astype(jnp.bfloat16)
    weighted = weighted + jnp.einsum(
        "hts,shd->thd", weights, key_value[1], preferred_element_type=jnp.float32
    )
    keep_total = keep_total + jnp.where(is_valid, jnp.sum(logarithmic_retention, axis=2), 0.0)
    return (weighted, keep_total)


def contract_rows(rows_in, weight):
    return lax.dot_general(
        rows_in, weight, (((1,), (1,)), ((), ())), preferred_element_type=jnp.float32
    )


def on_device(
    input_layer_rows,
    input_norm_gain,
    query_weight_attention,
    key_weight_attention,
    value_weight_attention,
    query_weight_recurrent,
    forget_weight_recurrent,
    value_weight_recurrent,
    gate_weight_recurrent,
    output_weight_attention,
    emitted_projection_linear_scan,
    score_offset,
    attention_norm_gain,
    recurrence_norm_gain,
    forget_floor,
    forget_offset,
    extra_log_decay,
):
    values = input_layer_rows[0].astype(jnp.float32)
    square_mean = jnp.mean(values * values, axis=-1, keepdims=True)
    normed = (values * lax.rsqrt(square_mean + epsilon) * input_norm_gain).astype(jnp.bfloat16)
    tokens = normed.shape[0]
    weights_in = (
        query_weight_attention,
        key_weight_attention,
        value_weight_attention,
        query_weight_recurrent,
        forget_weight_recurrent,
        value_weight_recurrent,
        gate_weight_recurrent,
    )
    pieces = sent_together(
        (
            weights_in[0],
            weights_in[1],
            weights_in[2],
            weights_in[3],
            weights_in[4],
            weights_in[5],
            weights_in[6],
        ),
        ("sp", "fs"),
        0,
        1,
    )
    projected = tuple(
        (jnp.dot(normed, weight, preferred_element_type=jnp.float32) for weight in pieces)
    )
    query_a, key_a, value_a, query_b, forget_b, input_b, gate_b = [
        column_block.astype(jnp.bfloat16) for column_block in projected
    ]
    out_a, out_b = sent_together(
        (output_weight_attention, emitted_projection_linear_scan), ("sp", "fs"), 0, 1
    )
    head_count = query_a.shape[1] // HEAD
    queries = query_a.reshape(tokens, head_count, HEAD)
    key_value = jnp.stack(
        [key_a.reshape(tokens, head_count, HEAD), value_a.reshape(tokens, head_count, HEAD)]
    )
    weighted = jnp.zeros((tokens, head_count, HEAD), jnp.float32)
    keep_total = jnp.zeros((head_count, tokens), jnp.float32)
    weighted, keep_total = stick_piece(
        queries, score_offset, weighted, keep_total, key_value, True, True
    )
    position = lax.axis_index("sp")
    seq_devices = lax.axis_size("sp")
    gathered = lax.all_gather(key_value, "sp", axis=1, tiled=True)

    def gathered_turn(turn_index, carried_state):
        weighted_now, keep_now = carried_state
        source = jnp.maximum(position - turn_index, 0) * tokens
        piece_pair = lax.dynamic_slice_in_dim(gathered, source, tokens, 1)
        return stick_piece(
            queries, score_offset, weighted_now, keep_now, piece_pair, False, position >= turn_index
        )

    weighted, keep_total = lax.fori_loop(1, seq_devices, gathered_turn, (weighted, keep_total))
    row_log_total = jnp.log(jnp.maximum(-jnp.expm1(keep_total), log_floor))[None]
    mixed_a = (
        head_norm(weighted, attention_norm_gain.reshape(head_count, HEAD))
        .reshape(tokens, head_count * HEAD)
        .astype(jnp.bfloat16)
    )
    forget_logits = forget_b.astype(jnp.float32) + forget_offset
    forget_log_value = (
        jnp.logaddexp(
            jnp.log(forget_floor), jnp.log1p(-forget_floor) + jax.nn.log_sigmoid(forget_logits)
        )
        + extra_log_decay[0]
    )
    key_in = (1.0 - forget_floor) * jax.nn.sigmoid(-forget_logits)
    query_rows_input = jax.nn.silu(query_b.astype(jnp.float32)).reshape(tokens, head_count, HEAD)
    value_in = input_b.astype(jnp.float32)
    fading_channel_groups = forget_log_value.reshape(tokens, head_count, HEAD)
    shaped = tuple(
        (
            array_in.reshape(tokens // BLOCK, BLOCK, head_count, HEAD)
            for array_in in (query_rows_input, forget_log_value, key_in, value_in)
        )
    )
    empty_state = jnp.zeros((head_count, HEAD, HEAD), jnp.float32)
    nearby_hidden_vector, local_out = lax.scan(recurrence_block, empty_state, shaped)
    local_out = local_out.reshape(tokens, head_count, HEAD)
    through = jnp.exp(jnp.sum(fading_channel_groups, axis=0))

    def chain_states(earlier, later):
        return (earlier[0] * later[0], later[0][:, :, None] * earlier[1] + later[1])

    identity = (jnp.ones_like(through), jnp.zeros_like(nearby_hidden_vector))
    unused_decay, incoming_state = entering(
        (through, nearby_hidden_vector), "sp", chain_states, identity
    )
    running_sum = jnp.cumsum(fading_channel_groups, axis=0)
    recurrent = local_out + jnp.einsum(
        "fby,bym->fbm",
        query_rows_input * jnp.exp(running_sum),
        incoming_state,
        precision=lax.Precision.HIGHEST,
    )
    gated_out = head_norm(recurrent, recurrence_norm_gain.reshape(head_count, HEAD)) * jax.nn.silu(
        gate_b.astype(jnp.float32).reshape(tokens, head_count, HEAD)
    )
    mixed_b = gated_out.reshape(tokens, head_count * HEAD).astype(jnp.bfloat16)
    summed = summed_on_arrival(
        (contract_rows(mixed_a, out_a) + contract_rows(mixed_b, out_b)).astype(jnp.bfloat16),
        "tp",
        0,
    )
    layer_out = summed.astype(jnp.bfloat16)[None]
    return (layer_out, row_log_total)


def solution(mesh):
    return jax.shard_map(
        on_device,
        mesh=mesh,
        in_specs=(
            P("fs", "sp", None),
            P(),
            P(("sp", "fs"), "tp"),
            P(("sp", "fs"), "tp"),
            P(("sp", "fs"), "tp"),
            P(("sp", "fs"), "tp"),
            P(("sp", "fs"), "tp"),
            P(("sp", "fs"), "tp"),
            P(("sp", "fs"), "tp"),
            P(("sp", "fs"), "tp"),
            P(("sp", "fs"), "tp"),
            P("tp"),
            P("tp"),
            P("tp"),
            P("tp"),
            P("tp"),
            P("fs", "sp", "tp"),
        ),
        out_specs=(P("fs", ("sp", "tp"), None), P("fs", "tp", "sp")),
        check_vma=False,
    )
```

profile of v0, /device:TPU:1, one launch (start us, length us, event | category | flops | bytes accessed | tf_op | source)
XLA Modules:
  0.0 408.0 jit_solution(14859455435213965333)
XLA Ops:
  12.9 1.5 fusion.41
  14.5 140.0 %all-gather.6.cloned.1.call-done = bf16[2048,896]{1,0:T(8,128)(2,1)} async-done(((bf16[32,896]{1,0:T(8,128)(2,1)}), bf16[2048,896]{1,0:T(8,128)(2,1)}) %all-gather.6.cloned.1.call-update) | async-done | bytes 3670032 | tf_op jit(solution)/shard_map/all_gather | solution.py:20
  154.5 1.9 convolution_convert_fusion.4
  156.4 1.6 convolution_convert_fusion.6
  160.1 1.5 convolution_convert_fusion.2
  161.7 1.6 divide_multiply_fusion
  163.3 1.7 fusion.107
  165.0 8.8 %while.43 = (s32[]{:T(128)}, f32[1,128,128]{2,1,0:T(8,128)S(1)}, f32[4,64,1,128]{3,1,2,0:T(8,128)S(1)}, f32[4,64,1,128]{3,1,2,0:T(8,128)S(1)}, f32[4,64,1,128]{3...) while((s32[]{:T(128)}, f32[1,128,128]{2,1,0:T(8,128)S(1)}, ...), condition=%wide.region_13.14_spmd.clone, body=%wide.region_10.13_spmd.clone.sunk | while | flops 34693120 | bytes 962680 | solution.py:236
  165.1 1.3 multiply_reduce_fusion.4
  167.3 1.3 multiply_reduce_fusion.4
  169.5 1.3 multiply_reduce_fusion.4
  171.7 1.3 multiply_reduce_fusion.4
  173.8 27.1 %all-gather.1 = bf16[16,129,128]{2,1,0:T(8,128)(2,1)S(1)} all-gather(bf16[1,129,128]{2,1,0:T(8,128)(2,1)S(1)} %maximum_bitcast_fusion), channel_id=2, replica_groups=mesh['sp'=16,'fs'=4,'tp'=8] {'sp'}, dimensions={0}, use_global_device_ids=true | all-gather | bytes 561408 | tf_op jit(solution)/shard_map/all_gather | solution.py:31
  201.2 1.5 convolution_convert_fusion.5
  203.1 2.3 fusion.68
  205.4 2.1 while.44
  208.6 18.3 %all-gather.8.cloned.1.call-done = bf16[2,4096,1,128]{3,1,2,0:T(8,128)(2,1)} async-done(((bf16[2,256,1,128]{3,1,2,0:T(8,128)(2,1)}), bf16[2,4096,1,128]{3,1,2,0:T(8,128)(2,1)}) %all-gather.8.cloned.1.call-update) | async-done | bytes 2097168 | tf_op jit(solution)/shard_map/all_gather | solution.py:201
  226.9 85.5 %while.42 = (s32[]{:T(128)}, f32[256,1,128]{0,2,1:T(8,128)S(1)}, f32[1,256]{1,0:T(1,128)S(1)}, s32[]{:T(128)}, bf16[2,4096,1,128]{3,1,2,0:T(8,128)(2,1)}, /*inde...) while((s32[]{:T(128)}, f32[256,1,128]{0,2,1:T(8,128)S(1)}, ...), condition=%wide.region_8.9_spmd, body=%wide.region_4.8_spmd.sunk | while | flops 43943176 | bytes 2841322 | solution.py:211
  226.9 1.9 fusion.140
  228.7 2.3 fusion.141
  231.5 1.0 fusion.143
  232.6 1.8 fusion.140
  234.4 2.3 fusion.141
  237.2 1.0 fusion.143
  238.3 1.8 fusion.140
  240.1 2.3 fusion.141
  242.9 1.0 fusion.143
  244.0 1.8 fusion.140
  245.8 2.3 fusion.141
  248.6 1.0 fusion.143
  249.7 1.8 fusion.140
  251.5 2.3 fusion.141
  254.3 1.0 fusion.143
  255.4 1.8 fusion.140
  257.2 2.3 fusion.141
  260.0 1.0 fusion.143
  261.1 1.8 fusion.140
  262.9 2.3 fusion.141
  265.7 1.0 fusion.143
  266.8 1.8 fusion.140
  268.6 2.3 fusion.141
  272.5 1.8 fusion.140
  274.3 2.3 fusion.141
  277.1 1.0 fusion.143
  278.2 1.8 fusion.140
  280.0 2.3 fusion.141
  282.8 1.0 fusion.143
  283.9 1.8 fusion.140
  285.7 2.3 fusion.141
  288.5 1.0 fusion.143
  289.6 1.8 fusion.140
  291.4 2.3 fusion.141
  294.2 1.0 fusion.143
  295.3 1.8 fusion.140
  297.1 2.3 fusion.141
  301.0 1.8 fusion.140
  302.8 2.3 fusion.141
  306.7 1.8 fusion.140
  308.5 2.3 fusion.141
  312.4 53.6 %all-gather.10.cloned.1.call-done = bf16[2048,256]{1,0:T(8,128)(2,1)} async-done(((bf16[32,256]{1,0:T(8,128)(2,1)}), bf16[2048,256]{1,0:T(8,128)(2,1)}) %all-gather.10.cloned.1.call-update) | async-done | bytes 1048592 | tf_op jit(solution)/shard_map/all_gather | solution.py:20
  366.1 1.6 fusion.55
  367.7 3.0 fusion.40
  370.7 15.0 %all-to-all-start = ((bf16[8,32,2048]{2,1,0:T(8,128)(2,1)}), bf16[8,32,2048]{2,1,0:T(8,128)(2,1)S(1)}, u32[]{:S(2)}, u32[]{:S(2)}) async-start(bf16[8,32,2048]{2,1,0:T(8,128)(2,1)} %bitcast.291), calls=%async_computation | async-start | bytes 2097152 | tf_op jit(solution)/shard_map/all_to_all | solution.py:69
  386.3 14.4 %all-to-all-done = bf16[8,32,2048]{2,1,0:T(8,128)(2,1)S(1)} async-done(((bf16[8,32,2048]{2,1,0:T(8,128)(2,1)}), bf16[8,32,2048]{2,1,0:T(8,128)(2,1)S(1)}, u32[]{:S(2)}, u32[]{:S(2)}) %all-to-all-start) | async-done | bytes 1048608 | tf_op jit(solution)/shard_map/all_to_all | solution.py:69
  (247 shorter events, 25.8 us)
Async XLA Ops:
  7.2 149.2 %copy-start = (bf16[1,256,2048]{2,1,0:T(8,128)(2,1)S(1)}, bf16[1,256,2048]{2,1,0:T(8,128)(2,1)}, u32[]{:S(2)}) copy-start(bf16[1,256,2048]{2,1,0:T(8,128)(2,1)} %param.23) | copy-start | bytes 3145732
  7.2 149.2 %copy-start.2 = (f32[2048]{0:T(1024)S(1)}, f32[2048]{0:T(1024)}, u32[]{:S(2)}) copy-start(f32[2048]{0:T(1024)} %param.24) | copy-start | bytes 24580
  7.2 147.3 %all-gather.6.cloned.1.call-start = ((), (), s32[]{:S(2)}) async-start(), calls=%async_computation.1 | async-start | bytes 3727360 | tf_op jit(solution)/shard_map/all_gather | solution.py:20
  12.2 0.6 copy-start.1
  12.9 214.0 %all-gather.8.cloned.1.call-start = ((), (), s32[]{:S(2)}) async-start(), calls=%async_computation.2 | async-start | bytes 2228224 | tf_op jit(solution)/shard_map/all_gather | solution.py:201
  156.4 2.3 copy-start.3
  156.4 2.3 copy-start.4
  156.4 3.0 copy-start.6
  158.6 207.4 %all-gather.10.cloned.1.call-start = ((), (), s32[]{:S(2)}) async-start(), calls=%async_computation.3 | async-start | bytes 1064960 | tf_op jit(solution)/shard_map/all_gather | solution.py:20
  161.6 1.6 copy-start.8
  161.6 1.6 copy-start.9
  226.9 139.2 %copy-start.7 = (f32[128]{0:T(128)S(1)}, f32[128]{0:T(128)}, u32[]{:S(2)}) copy-start(f32[128]{0:T(128)} %param.35) | copy-start | bytes 1540
  312.4 55.3 %copy-start.5 = (f32[128]{0:T(128)S(1)}, f32[128]{0:T(128)}, u32[]{:S(2)}) copy-start(f32[128]{0:T(128)} %param.36) | copy-start | bytes 1540
  370.7 30.0 %all-to-all-start = ((bf16[8,32,2048]{2,1,0:T(8,128)(2,1)}), bf16[8,32,2048]{2,1,0:T(8,128)(2,1)S(1)}, u32[]{:S(2)}, u32[]{:S(2)}) async-start(bf16[8,32,2048]{2,1,0:T(8,128)(2,1)} %bitcast.291), calls=%async_computation | async-start | bytes 2097152 | tf_op jit(solution)/shard_map/all_to_all | solution.py:69
Sparse Core Ops, SparseCore 0:
  13.0 141.4 all-gather.5
  158.8 68.0 all-gather.7
  229.8 136.2 all-gather.9
where the time goes:
time: 410 us; the launch traced here: 408 us
  waiting for transfers between devices  226 us (55%)
  matrix products  61.3 us (15%)
  other arithmetic  55.1 us (13%)
  blocking collectives  27.1 us (7%)
  starting transfers between devices  15.1 us (4%)
  between operations  14.7 us (4%)
  local copies, waits for them, and re-layouts  6.39 us (2%)
    all_gather x2, waiting for transfers between devices, sent_together(): lax.all_gather(both, axis, axis=dim, tiled=True)  194 us
    another operation x34, other arithmetic  37.4 us
    dot_general x16, matrix products, stick_piece(): jnp.einsum('thd,shd->hts', queries, key_value[0], preferred_element_type=...  28 us
    all_gather x1, blocking collectives, collected_together(): both, at, found = (lax.all_gather(jnp.concatenate(lines), axis), 0, {})  27.1 us
    all_gather x1, waiting for transfers between devices, on_device(): gathered = lax.all_gather(key_value, 'sp', axis=1, tiled=True)  18.3 us
    dot_general x16, matrix products, stick_piece(): jnp.einsum('hts,shd->thd', weights, key_value[1], preferred_element_type=...  15.9 us
    all_to_all x1, starting transfers between devices, summed_on_arrival(): tiles = lax.all_to_all(in_blocks(shard, dim, size), axis, 0, 0, tiled=True)  15 us
    all_to_all x1, waiting for transfers between devices, summed_on_arrival(): tiles = lax.all_to_all(in_blocks(shard, dim, size), axis, 0, 0, tiled=True)  14.4 us
  transfers between devices with their start and end apart: 4, of which 4 were waited for; matrix products, arithmetic and copies ran while one was open for 26% of the time, Pallas kernels for 0%

commit v1 on v0

v1 whole, which is shorter than its diff:
```python
import jax
import jax.numpy as jnp
from jax import lax
from jax.experimental import pallas as pl
from jax.experimental.pallas import tpu as pltpu
from jax.sharding import PartitionSpec as P

HEAD = 128
ROWS = 32
TILE = 16

epsilon = 1e-06
log_floor = 0.05
F32 = jnp.float32
BF16 = jnp.bfloat16
INTERPRET = False


def vmem_call(kernel, outs, n_in, smem=()):
    specs = [
        pl.BlockSpec(memory_space=pltpu.SMEM if k in smem else pltpu.VMEM) for k in range(n_in)
    ]
    return pl.pallas_call(
        kernel,
        out_shape=outs,
        in_specs=specs,
        out_specs=jax.tree.map(lambda _: pl.BlockSpec(memory_space=pltpu.VMEM), outs),
        interpret=INTERPRET,
    )


def dot(a, b, dims=((1,), (0,))):
    return lax.dot_general(a, b, (dims, ((), ())), preferred_element_type=F32)


def parts(a):
    high = a.astype(BF16)
    return high, (a - high.astype(F32)).astype(BF16)


def dot_left(a, b, dims=((1,), (0,))):
    high, low = parts(a)
    return dot(high, b, dims) + dot(low, b, dims)


def dot_both(a, b, dims):
    a_high, a_low = parts(a)
    b_high, b_low = parts(b)
    return dot(a_high, b_high, dims) + (dot(a_high, b_low, dims) + dot(a_low, b_high, dims))


def times_weight(normed, weight_ref):
    fs, sp, rows, cols = weight_ref.shape
    step = 2 if sp % 2 == 0 else 1
    total = None
    for s in range(0, sp, step):
        piece = jnp.concatenate(
            [weight_ref[:, s + k].reshape(fs * rows, cols) for k in range(step)], axis=0
        )
        width = step * fs * rows
        term = dot(normed[:, s * fs * rows : s * fs * rows + width], piece)
        total = term if total is None else total + term
    return total


def norm_project_kernel(x_ref, gain_ref, weight_ref, normed_ref, out_ref):
    values = x_ref[...].astype(F32)
    square_mean = jnp.mean(values * values, axis=-1, keepdims=True)
    normed = (values * lax.rsqrt(square_mean + epsilon) * gain_ref[...]).astype(BF16)
    normed_ref[...] = normed
    out_ref[...] = times_weight(normed_ref, weight_ref).astype(BF16)


def local_recurrence_kernel(
    normed_ref,
    weight_ref,
    floor_ref,
    offset_ref,
    extra_ref,
    query_a_ref,
    inner_ref,
    query_decayed_ref,
    gate_ref,
    state_ref,
):
    projected = times_weight(normed_ref, weight_ref).astype(BF16)
    columns = [projected[:, k * HEAD : (k + 1) * HEAD] for k in range(5)]
    query_a_ref[...] = columns[0]
    query_b = columns[1].astype(F32)
    query = query_b / (1.0 + jnp.exp(-query_b))
    value = columns[3]
    gate_b = columns[4].astype(F32)
    gate_ref[...] = gate_b / (1.0 + jnp.exp(-gate_b))
    u = columns[2].astype(F32) + offset_ref[...]
    key = (1.0 - floor_ref[...]) / (1.0 + jnp.exp(u))
    log_forget = jnp.log(1.0 - key) + extra_ref[...]
    length = log_forget.shape[0]
    row = lax.broadcasted_iota(jnp.int32, (length, length), 0)
    col = lax.broadcasted_iota(jnp.int32, (length, length), 1)
    lower = (row >= col).astype(BF16)
    high = log_forget.astype(BF16)
    rest = log_forget - high.astype(F32)
    middle = rest.astype(BF16)
    low = (rest - middle.astype(F32)).astype(BF16)
    running = dot(lower, high) + (dot(lower, middle) + dot(lower, low))
    position = lax.broadcasted_iota(jnp.int32, (length, 1), 0)
    pairwise = jnp.where(row == col, dot_both(query, key, ((1,), (1,))), 0.0)
    half = 1
    while half < length:
        block = 2 * half
        if block >= 8:
            boundary = running.reshape(length // block, block, HEAD)[:, half - 1 : half]
            boundary = jnp.broadcast_to(boundary, (length // block, block, HEAD)).reshape(
                length, HEAD
            )
        else:
            tiles = running.reshape(length // 8, 8, HEAD)
            inside = lax.broadcasted_iota(jnp.int32, (1, 8, 1), 1) // block
            boundary = jnp.zeros_like(tiles)
            for k in range(8 // block):
                at = k * block + half - 1
                boundary = jnp.where(inside == k, tiles[:, at : at + 1], boundary)
            boundary = boundary.reshape(length, HEAD)
        second = (position // half) % 2 == 1
        after = jnp.where(second, query * jnp.exp(running - boundary), 0.0)
        before = jnp.where(second, 0.0, key * jnp.exp(boundary - running))
        chosen = (row // block == col // block) & (row // half != col // half) & (row > col)
        pairwise = jnp.where(chosen, dot_both(after, before, ((1,), (1,))), pairwise)
        half = block
    inner_ref[...] = dot_left(pairwise, value)
    final = running[length - 1 : length]
    query_decayed_ref[...] = query * jnp.exp(running)
    key_high, key_low = parts(key * jnp.exp(final - running))
    state = dot(value, key_high, ((0,), (0,))) + dot(value, key_low, ((0,), (0,)))
    state_ref[0:HEAD] = state.astype(BF16)
    state_ref[HEAD : HEAD + TILE] = jnp.broadcast_to(jnp.exp(final), (TILE, HEAD)).astype(BF16)


def mixed_b_kernel(
    rank_ref, message_ref, inner_ref, query_decayed_ref, gate_ref, gain_ref, out_ref
):
    def chain(k, state):
        decay = message_ref[k, HEAD : HEAD + TILE].astype(F32)[0:1]
        return decay * state + message_ref[k, 0:HEAD].astype(F32)

    state = lax.fori_loop(0, rank_ref[0], chain, jnp.zeros((HEAD, HEAD), F32))
    recurrent = inner_ref[...] + dot_both(query_decayed_ref[...], state, ((1,), (1,)))
    square_mean = jnp.mean(recurrent * recurrent, axis=-1, keepdims=True)
    mixed = recurrent * lax.rsqrt(square_mean + epsilon) * gain_ref[...] * gate_ref[...]
    out_ref[...] = mixed.astype(BF16)


def attention_kernel(
    rank_ref,
    shift_ref,
    query_ref,
    key_value_ref,
    gain_ref,
    mixed_b_ref,
    weight_ref,
    out_ref,
    total_ref,
):
    rank = rank_ref[0]
    shift = shift_ref[0]
    query = query_ref[...]
    length = query.shape[0]
    row = lax.broadcasted_iota(jnp.int32, (length, length), 0)
    col = lax.broadcasted_iota(jnp.int32, (length, length), 1)
    strict = row > col
    suffix = (row >= col).astype(BF16)

    def piece(source, total, is_own):
        start = pl.multiple_of(source * length, length)
        key = key_value_ref[pl.ds(start, length), 0:HEAD]
        value = key_value_ref[pl.ds(start, length), HEAD : 2 * HEAD]
        scores = dot(query, key, ((1,), (1,))) * HEAD ** (-0.5) + shift
        softplus = jnp.maximum(scores, 0.0) + jnp.log(1.0 + jnp.exp(-jnp.abs(scores)))
        if is_own:
            softplus = jnp.where(strict, softplus, 0.0)
        spent = dot_left(softplus, suffix) + total
        weights = jnp.exp(scores - spent)
        if is_own:
            weights = jnp.where(strict, weights, 0.0)
        return dot(weights.astype(BF16), value), spent[:, 0:1]

    carry = piece(rank, 0.0, True)

    def earlier(k, carry):
        weighted, total = carry
        more, total = piece(rank - 1 - k, total, False)
        return weighted + more, total

    weighted, total = lax.fori_loop(0, rank, earlier, carry)
    total_row = jnp.transpose(jnp.broadcast_to(total, (length, HEAD)))[0:1]
    total_ref[...] = jnp.log(jnp.maximum(1.0 - jnp.exp(-total_row), log_floor))
    square_mean = jnp.mean(weighted * weighted, axis=-1, keepdims=True)
    mixed_a = (weighted * lax.rsqrt(square_mean + epsilon) * gain_ref[...]).astype(BF16)
    mixed = jnp.concatenate([mixed_a, mixed_b_ref[...]], axis=1)
    fs, sp = weight_ref.shape[:2]
    width = fs * ROWS
    for s in range(sp):
        both = jnp.concatenate(
            [weight_ref[:, s, k].reshape(width, HEAD) for k in range(2)], axis=1
        )
        out_ref[:, s * width : (s + 1) * width] = dot(mixed, both, ((1,), (1,))).astype(BF16)


def over_fs(shard):
    size = lax.axis_size("fs")
    copies = jnp.broadcast_to(shard[None], (size, *shard.shape))
    return lax.all_to_all(copies, "fs", 0, 0, tiled=True)


def on_device(
    input_layer_rows,
    input_norm_gain,
    query_weight_attention,
    key_weight_attention,
    value_weight_attention,
    query_weight_recurrent,
    forget_weight_recurrent,
    value_weight_recurrent,
    gate_weight_recurrent,
    output_weight_attention,
    emitted_projection_linear_scan,
    score_offset,
    attention_norm_gain,
    recurrence_norm_gain,
    forget_floor,
    forget_offset,
    extra_log_decay,
):
    x = input_layer_rows[0]
    tokens, width = x.shape
    sp, fs, tp = (lax.axis_size(name) for name in ("sp", "fs", "tp"))
    rank = lax.axis_index("sp").astype(jnp.int32).reshape(1)
    local = jnp.concatenate(
        (
            key_weight_attention,
            value_weight_attention,
            query_weight_attention,
            query_weight_recurrent,
            forget_weight_recurrent,
            value_weight_recurrent,
            gate_weight_recurrent,
        ),
        axis=1,
    )
    column = lax.all_gather(local, "sp")
    first = over_fs(column[:, :, : 2 * HEAD])
    normed, key_value = vmem_call(
        norm_project_kernel,
        (
            jax.ShapeDtypeStruct((tokens, width), BF16),
            jax.ShapeDtypeStruct((tokens, 2 * HEAD), BF16),
        ),
        3,
    )(x, input_norm_gain.reshape(1, width), first)
    everything = lax.all_gather(key_value, "sp", axis=0, tiled=True)
    column, key_value = lax.optimization_barrier((column, key_value))
    second = over_fs(column[:, :, 2 * HEAD :])
    small = jax.ShapeDtypeStruct((tokens, HEAD), F32)
    query_a, inner, query_decayed, gate, state = vmem_call(
        local_recurrence_kernel,
        (
            jax.ShapeDtypeStruct((tokens, HEAD), BF16),
            small,
            small,
            small,
            jax.ShapeDtypeStruct((HEAD + TILE, HEAD), BF16),
        ),
        5,
    )(
        normed,
        second,
        forget_floor.reshape(1, HEAD),
        forget_offset.reshape(1, HEAD),
        extra_log_decay[0],
    )
    message = lax.all_gather(
        jnp.concatenate((state, output_weight_attention, emitted_projection_linear_scan), axis=0),
        "sp",
    )
    out_weights = over_fs(message[:, HEAD + TILE :].reshape(sp, 2, ROWS, HEAD))
    mixed_b = vmem_call(mixed_b_kernel, jax.ShapeDtypeStruct((tokens, HEAD), BF16), 6, (0,))(
        rank, message, inner, query_decayed, gate, recurrence_norm_gain.reshape(1, HEAD)
    )
    projected, row_log_total = vmem_call(
        attention_kernel,
        (
            jax.ShapeDtypeStruct((tokens, width), BF16),
            jax.ShapeDtypeStruct((1, tokens), F32),
        ),
        7,
        (0, 1),
    )(
        rank,
        score_offset,
        query_a,
        everything,
        attention_norm_gain.reshape(1, HEAD),
        mixed_b,
        out_weights,
    )
    tiles = lax.all_to_all(projected.reshape(tp, tokens // tp, width), "tp", 0, 0, tiled=True)
    layer_out = jnp.sum(tiles.astype(F32), axis=0).astype(BF16)
    return (layer_out[None], row_log_total[None])


def solution(mesh):
    weight = P(("sp", "fs"), "tp")
    return jax.shard_map(
        on_device,
        mesh=mesh,
        in_specs=(
            P("fs", "sp", None),
            P(),
            *(weight for _ in range(9)),
            *(P("tp") for _ in range(5)),
            P("fs", "sp", "tp"),
        ),
        out_specs=(P("fs", ("sp", "tp"), None), P("fs", "tp", "sp")),
        check_vma=False,
    )
```

time: 410 us -> 192 us (0.47)
  waiting for transfers between devices: 226 us -> 6.81 us
  blocking collectives: 27.1 us -> 141 us
  matrix products: 61.3 us -> 0 us
  other arithmetic: 55.1 us -> 1.59 us
  Pallas kernels: 0 us -> 15.1 us
  starting transfers between devices: 15.1 us -> 3.55 us
    all_gather x3 -> x1, waiting for transfers between devices: 212 us -> 0.01 us  [on_device(): everything = lax.all_gather(key_value, 'sp', axis=0, tiled=True)]
    all_to_all x0 -> x3, blocking collectives: none -> 73.6 us  [the longest x2 39.8 us: over_fs(): return lax.all_to_all(copies, 'fs', 0, 0, tiled=True)]
    dot_general x53 -> x0, matrix products: 61.3 us -> none  [the longest x16 28 us: stick_piece(): jnp.einsum('thd,shd->hts', queries, key_value[0], preferred_element_type=...]
    all_gather x1 -> x2, blocking collectives: 27.1 us -> 67 us  [the longest x1 34.5 us: on_device(): column = lax.all_gather(local, 'sp')]
    another operation x39 -> x0, other arithmetic: 38.4 us -> none
    pallas_call x0 -> x4, Pallas kernels: none -> 15.1 us  [the longest x1 5.46 us: on_device(): vmem_call(local_recurrence_kernel, (jax.ShapeDtypeStruct((tokens, HEAD),...]
    all_to_all x1, starting transfers between devices: 15 us -> 3.51 us  [over_fs(): return lax.all_to_all(copies, 'fs', 0, 0, tiled=True)]
    all_to_all x1, waiting for transfers between devices: 14.4 us -> 6.79 us  [over_fs(): return lax.all_to_all(copies, 'fs', 0, 0, tiled=True)]
  transfers between devices with their start and end apart: 4 -> 2, of which waited for: 4 -> 1; matrix products, arithmetic and copies ran while one was open for 26% -> 1% of each run, Pallas kernels for 0% -> 4%
where the time goes in v1:
time: 192 us; the launch traced here: 190 us
  blocking collectives  141 us (73%)
  Pallas kernels  15.1 us (8%)
  between operations  14.7 us (8%)
  local copies, waits for them, and re-layouts  7.57 us (4%)
  waiting for transfers between devices  6.81 us (4%)
  starting transfers between devices  3.55 us (2%)
    all_to_all x2, blocking collectives, over_fs(): return lax.all_to_all(copies, 'fs', 0, 0, tiled=True)  39.8 us
    all_gather x1, blocking collectives, on_device(): column = lax.all_gather(local, 'sp')  34.5 us
    all_to_all x1, blocking collectives, on_device(): lax.all_to_all(projected.reshape(tp, tokens // tp, width), 'tp', 0, 0, ti...  33.7 us
    all_gather x1, blocking collectives, on_device(): lax.all_gather(jnp.concatenate((state, output_weight_attention, emitted_p...  32.4 us
    all_to_all x1, waiting for transfers between devices, over_fs(): return lax.all_to_all(copies, 'fs', 0, 0, tiled=True)  6.79 us
    pallas_call x1, Pallas kernels, on_device(): vmem_call(local_recurrence_kernel, (jax.ShapeDtypeStruct((tokens, HEAD),...  5.46 us
    unnamed x14, local copies, waits for them, and re-layouts  5.19 us
    pallas_call x1, Pallas kernels, on_device(): vmem_call(attention_kernel, (jax.ShapeDtypeStruct((tokens, width), BF16),...  4.3 us
  transfers between devices with their start and end apart: 2, of which 1 were waited for; matrix products, arithmetic and copies ran while one was open for 1% of the time, Pallas kernels for 4%

profile of v1, /device:TPU:1, one launch (start us, length us, event | category | flops | bytes accessed | tf_op | source)
XLA Modules:
  0.0 189.9 jit_solution(4705622725089801103)
XLA Ops:
  7.2 0.0 all-gather.4.cloned.1.call-start
  7.2 0.7 constant_dynamic-update-slice_fusion.6
  7.9 0.7 constant_dynamic-update-slice_fusion.5
  8.6 0.7 constant_dynamic-update-slice_fusion.4
  9.3 0.7 constant_dynamic-update-slice_fusion.3
  10.0 0.7 constant_dynamic-update-slice_fusion.2
  10.7 0.7 constant_dynamic-update-slice_fusion.1
  11.4 0.7 constant_dynamic-update-slice_fusion
  12.1 34.5 %all-gather = bf16[512,896]{1,0:T(8,128)(2,1)S(1)} all-gather(bf16[32,896]{1,0:T(8,128)(2,1)S(1)} %constant_dynamic-update-slice_fusion), channel_id=2, replica_groups=mesh['sp'=16,'fs'=4,'tp'=8] {'sp'}, dimensions={0}, use_global_device_ids=true | all-gather | bytes 974848 | tf_op jit(solution)/shard_map/all_gather | solution.py:250
  46.7 0.1 broadcast_in_dim.12
  46.8 13.8 %all_to_all.20.weight_ref = bf16[4,16,32,256]{3,2,1,0:T(8,128)(2,1)} all-to-all(bf16[4,16,32,256]{3,2,1,0:T(8,128)(2,1)S(1)} %broadcast_in_dim.12), channel_id=1, replica_groups=mesh['sp'=16,'fs'=4,'tp'=8] {'fs'}, dimensions={0} | all-to-all | bytes 2097152 | tf_op jit(solution)/shard_map/all_to_all | solution.py:212
  60.7 3.1 %shard_map.176 = (bf16[256,2048]{1,0:T(8,128)(2,1)}, bf16[256,256]{1,0:T(8,128)(2,1)}) custom-call(bf16[256,2048]{1,0:T(8,128)(2,1)} %bitcast.19, f32[1,2048]{1,0:T(1,128)} %bitcast.23, bf16[4,16,32,256]{3,2,1,0:T(8,128)(2,1)} %all_to_all.20.weight_ref), custom_call_target="tpu_custom_call" | custom-call | tf_op jit(solution)/shard_map/pallas_call | solution.py:252
  63.8 0.0 all-gather.4.cloned.1.call-update
  63.8 0.1 slice.10
  63.9 0.2 broadcast_in_dim.26
  64.1 26.0 %all_to_all.21.weight_ref = bf16[4,16,32,640]{3,2,1,0:T(8,128)(2,1)} all-to-all(bf16[4,16,32,640]{3,2,1,0:T(8,128)(2,1)S(1)} %broadcast_in_dim.26), channel_id=1, replica_groups=mesh['sp'=16,'fs'=4,'tp'=8] {'fs'}, dimensions={0} | all-to-all | bytes 5242880 | tf_op jit(solution)/shard_map/all_to_all | solution.py:212
  90.1 0.0 copy-start.2
  90.1 0.0 copy-start.3
  90.1 5.5 %shard_map.177 = (bf16[256,128]{1,0:T(8,128)(2,1)}, f32[256,128]{1,0:T(8,128)}, f32[256,128]{1,0:T(8,128)}, f32[256,128]{1,0:T(8,128)}, bf16[144,128]{1,0:T(8,128)(2,1)}) custom-call(bf16[256,2048]{1,0:T(8,128)(2,1)} %get-tuple-element.12.normed_ref, bf16[4,16,32,640]{3,2,1,0:T(8,128)(2,1)} %all_to_all.21.weight_ref, f32[1,128]{1,0:T(1,128)} %bitcast.24, ...), custom_call_target="tpu_custom_call" | custom-call | tf_op jit(solution)/shard_map/pallas_call | solution.py:264
  95.6 0.0 copy-done.2
  95.6 0.0 copy-done.3
  95.6 0.8 pad_maximum_fusion
  96.4 32.4 %all-gather.1 = bf16[3328,128]{1,0:T(8,128)(2,1)S(1)} all-gather(bf16[208,128]{1,0:T(8,128)(2,1)S(1)} %pad_maximum_fusion), channel_id=3, replica_groups=mesh['sp'=16,'fs'=4,'tp'=8] {'sp'}, dimensions={0}, use_global_device_ids=true | all-gather | bytes 905216 | tf_op jit(solution)/shard_map/all_gather | solution.py:281
  128.8 0.0 copy-start
  128.8 1.2 broadcast_in_dim.28
  130.0 3.5 %all-to-all-start.2 = ((bf16[4,16,2,32,128]{4,3,2,1,0:T(8,128)(2,1)}), bf16[4,16,2,32,128]{4,3,2,1,0:T(8,128)(2,1)S(1)}, u32[]{:S(2)}, u32[]{:S(2)}) async-start(bf16[4,16,2,32,128]{4,3,2,1,0:T(8,128)(2,1)} %broadcast_in_dim.28), calls=%async_computation.2 | async-start | bytes 2097152 | tf_op jit(solution)/shard_map/all_to_all | solution.py:212
  134.2 0.0 copy-done
  134.2 2.3 %shard_map.178.mixed_b_ref = bf16[256,128]{1,0:T(8,128)(2,1)} custom-call(s32[1]{0:T(128)} %bitcast.rank_ref, bf16[16,208,128]{2,1,0:T(8,128)(2,1)} %bitcast.15, f32[256,128]{1,0:T(8,128)} %get-tuple-element.17.inner_ref, f32[256,128]{1,0:T(8,128)} %get-tuple-element.18.query_decayed_ref, f32[256,128]{1,0:T(8,128)} %get-tuple-element.19.gate_ref, ...), custom_call_target="tpu_custom_call" | custom-call | tf_op jit(solution)/shard_map/pallas_call | solution.py:286
  136.5 6.8 %all-to-all-done.2.weight_ref = bf16[4,16,2,32,128]{4,3,2,1,0:T(8,128)(2,1)S(1)} async-done(((bf16[4,16,2,32,128]{4,3,2,1,0:T(8,128)(2,1)}), bf16[4,16,2,32,128]{4,3,2,1,0:T(8,128)(2,1)S(1)}, u32[]{:S(2)}, u32[]{:S(2)}) %all-to-all-start.2) | async-done | bytes 1048608 | tf_op jit(solution)/shard_map/all_to_all | solution.py:212
  143.2 0.0 copy-start.1
  143.2 0.0 all-gather.4.cloned.1.call-done.key_value_ref
  143.3 1.0 copy-done.1
  144.2 4.3 %shard_map.179 = (bf16[256,2048]{1,0:T(8,128)(2,1)}, f32[1,256]{1,0:T(1,128)}) custom-call(s32[1]{0:T(128)} %bitcast.rank_ref, f32[1]{0:T(128)S(6)} %copy.25.shift_ref, bf16[256,128]{1,0:T(8,128)(2,1)} %get-tuple-element.15.query_ref, bf16[4096,256]{1,0:T(8,128)(2,1)} %all-gather.4.cloned.1.call-done.key_value_ref, f32[1,128]{1,0:T(1,128)} %bitcast.27, ...), custom_call_target="tpu_custom_call" | custom-call | tf_op jit(solution)/shard_map/pallas_call | solution.py:289
  148.5 33.7 %all_to_all.22 = bf16[8,32,2048]{2,1,0:T(8,128)(2,1)S(1)} all-to-all(bf16[8,32,2048]{2,1,0:T(8,128)(2,1)} %bitcast.20), channel_id=1, replica_groups=mesh['sp'=16,'fs'=4,'tp'=8] {'tp'}, dimensions={0} | all-to-all | bytes 2097152 | tf_op jit(solution)/shard_map/all_to_all | solution.py:306
  182.2 0.8 reduce_sum.12
  (2 shorter events, 0.0 us)
Async XLA Ops:
  7.2 136.1 %all-gather.4.cloned.1.call-start = ((), (), s32[]{:S(2)}) async-start(), calls=%async_computation.4 | async-start | bytes 2228224 | tf_op jit(solution)/shard_map/all_gather | solution.py:260
  90.1 5.5 %copy-start.2 = (bf16[32,128]{1,0:T(8,128)(2,1)S(1)}, bf16[32,128]{1,0:T(8,128)(2,1)}, u32[]{:S(2)}) copy-start(bf16[32,128]{1,0:T(8,128)(2,1)} %param.27) | copy-start | bytes 24580
  90.1 5.5 %copy-start.3 = (bf16[32,128]{1,0:T(8,128)(2,1)S(1)}, bf16[32,128]{1,0:T(8,128)(2,1)}, u32[]{:S(2)}) copy-start(bf16[32,128]{1,0:T(8,128)(2,1)} %param.26) | copy-start | bytes 24580
  128.8 5.4 %copy-start = (bf16[3328,128]{1,0:T(8,128)(2,1)}, bf16[3328,128]{1,0:T(8,128)(2,1)S(1)}, u32[]{:S(2)}) copy-start(bf16[3328,128]{1,0:T(8,128)(2,1)S(1)} %all-gather.1) | copy-start | bytes 2555908
  130.0 13.2 %all-to-all-start.2 = ((bf16[4,16,2,32,128]{4,3,2,1,0:T(8,128)(2,1)}), bf16[4,16,2,32,128]{4,3,2,1,0:T(8,128)(2,1)S(1)}, u32[]{:S(2)}, u32[]{:S(2)}) async-start(bf16[4,16,2,32,128]{4,3,2,1,0:T(8,128)(2,1)} %broadcast_in_dim.28), calls=%async_computation.2 | async-start | bytes 2097152 | tf_op jit(solution)/shard_map/all_to_all | solution.py:212
  143.2 1.0 copy-start.1
Sparse Core Ops, SparseCore 0:
  63.9 68.3 all-gather.3
